TPU v7x, 32 devices: a whole 2x2x4 slice. The times are simulated.
32 devices in a mesh: sp: 8 (over z, x), tp: 4 (over y, core).
Axes of the slice: x: 2, y: 2, z: 4, core: 2. Of those that a mesh axis runs over, the one named last changes fastest.
Arguments:
- hidden_in: bfloat16 [2048, 2048], P('sp'), may hold values from -6 to 6
- cotangent: bfloat16 [2048, 2048], P('sp'), may hold values from -6 to 6
- routes: int32 [2048, 2], P('sp'), may hold values from 0 to 7, all different within a row; in each aligned block of 256 rows (0 to 255, 256 to 511, ...) at most 96 rows name the same one
- routing_weights: float32 [2048, 2], P('sp'), may hold values from 0.1 to 1
- w_gate: bfloat16 [8, 2048, 1024], P('sp', None, 'tp'), may hold values from -0.125 to 0.125
- w_up: bfloat16 [8, 2048, 1024], P('sp', None, 'tp'), may hold values from -0.125 to 0.125
- w_down: bfloat16 [8, 1024, 2048], P('sp', 'tp'), may hold values from -0.1875 to 0.1875
- b_gate: bfloat16 [2048, 1024], P('sp', 'tp'), may hold values from -6 to 6
- c_gate: bfloat16 [2048, 1024], P('sp', 'tp'), may hold values from -6 to 6
- x_in: bfloat16 [2048, 1024], P('sp', 'tp'), may hold values from -6 to 6
- taps: bfloat16 [3, 1024], P(None, 'tp'), may hold values from -3 to 3
- w_out: bfloat16 [2048, 1024], P(None, 'tp'), may hold values from -0.1875 to 0.1875
Outputs:
- grad_gate: bfloat16 [8, 2048, 1024], P('sp', None, 'tp')
- grad_up: bfloat16 [8, 2048, 1024], P('sp', None, 'tp')
- grad_down: bfloat16 [8, 1024, 2048], P('sp', 'tp')
- out_proj_grad: float32 [2048, 1024], P('sp', 'tp')
- residual_grad: bfloat16 [2048, 2048], P('sp', 'tp')
- grad_b: bfloat16 [2048, 1024], P('sp', 'tp')
- grad_c: bfloat16 [2048, 1024], P('sp', 'tp')
- grad_x: bfloat16 [2048, 1024], P('sp', 'tp')
Inputs may be any that keep to these rules, and one draw needn't show every extreme that they name: `routes`: each row names 2 different experts. Among the rows of one index of sp no expert is named more than 96 times, a bound that some block reaches in some of them.
All inputs are finite; a program needn't handle non-finite values.
Results may differ from a plain program's by a relative error of at most 0.01.
Values may be sent and summed in bfloat16 or wider, within the bound.
A program may use at most 64 MiB of HBM per device.

v0:
```python
import jax
import jax.numpy as jnp
from jax import lax
from jax.sharding import PartitionSpec as P


def from_behind(x, axis, by):
    devices = lax.axis_size(axis)
    pairs = [(i, i + by) for i in range(devices) if 0 <= i + by < devices]
    return lax.ppermute(x, axis, pairs)


def per_device(
    hidden_in,
    cotangent,
    routes,
    routing_weights,
    w_gate,
    w_up,
    w_down,
    b_gate,
    c_gate,
    x_in,
    taps,
    w_out,
):
    tok_rows, model_width = hidden_in.shape
    top_k = routes.shape[1]
    local_experts = w_gate.shape[0]
    sp_size = lax.axis_size("sp")
    tp_size = lax.axis_size("tp")
    experts = local_experts * sp_size
    capacity = 3 * tok_rows * top_k // (2 * experts)
    slot_count = tok_rows * top_k
    feature_share = model_width // tp_size
    share_offset = lax.axis_index("tp") * feature_share
    flat_ids = routes.reshape(-1)
    onehot = (flat_ids[:, None] == jnp.arange(experts, dtype=jnp.int32)[None, :]).astype(jnp.int32)
    before = jnp.cumsum(onehot, axis=0) - onehot
    position = jnp.sum(before * onehot, axis=1)
    target = flat_ids * capacity + position
    source = (
        jnp.full((experts * capacity,), slot_count, jnp.int32)
        .at[target]
        .set(jnp.arange(slot_count, dtype=jnp.int32))
    )
    filled = source < slot_count
    clipped = jnp.minimum(source, slot_count - 1)
    token_of = clipped // top_k
    weight_of = jnp.where(filled, routing_weights.reshape(-1)[clipped], 0.0)
    rows_src = lax.dynamic_slice_in_dim(hidden_in, share_offset, feature_share, 1)
    cot_src = lax.dynamic_slice_in_dim(cotangent, share_offset, feature_share, 1)
    send_rows = jnp.where(filled[:, None], rows_src[token_of], jnp.zeros((), jnp.bfloat16))
    send_rows = send_rows.reshape(experts, capacity, -1)
    send_cot = (weight_of[:, None] * cot_src[token_of].astype(jnp.float32)).astype(jnp.bfloat16)
    send_cot = send_cot.reshape(experts, capacity, -1)
    part_rows, part_cot = (
        lax.all_to_all(send_rows, "sp", split_axis=0, concat_axis=1, tiled=True),
        lax.all_to_all(send_cot, "sp", split_axis=0, concat_axis=1, tiled=True),
    )
    rows_h, rows_s = (
        lax.all_gather(part_rows, "tp", axis=2, tiled=True),
        lax.all_gather(part_cot, "tp", axis=2, tiled=True),
    )
    pre_gate = jnp.einsum("erd,edf->erf", rows_h, w_gate, preferred_element_type=jnp.float32)
    pre_up = jnp.einsum("erd,edf->erf", rows_h, w_up, preferred_element_type=jnp.float32)
    sigma = jax.nn.sigmoid(pre_gate)
    silu_gate = pre_gate * sigma
    hid = (silu_gate * pre_up).astype(jnp.bfloat16)
    d_hid = jnp.einsum("erd,efd->erf", rows_s, w_down, preferred_element_type=jnp.float32)
    d_up = (d_hid * silu_gate).astype(jnp.bfloat16)
    d_pre = (d_hid * pre_up * sigma * (1.0 + pre_gate * (1.0 - sigma))).astype(jnp.bfloat16)
    grad_down = jnp.einsum("erf,erd->efd", hid, rows_s, preferred_element_type=jnp.float32).astype(
        jnp.bfloat16
    )
    grad_gate = jnp.einsum(
        "erd,erf->edf", rows_h, d_pre, preferred_element_type=jnp.float32
    ).astype(jnp.bfloat16)
    grad_up = jnp.einsum("erd,erf->edf", rows_h, d_up, preferred_element_type=jnp.float32).astype(
        jnp.bfloat16
    )
    partial_grad = jnp.einsum("erf,edf->erd", d_pre, w_gate, preferred_element_type=jnp.float32)
    partial_grad = partial_grad + jnp.einsum(
        "erf,edf->erd", d_up, w_up, preferred_element_type=jnp.float32
    )
    partial_low = partial_grad.astype(jnp.bfloat16)
    shared_rows = (
        lax.psum_scatter(partial_low, "tp", scatter_dimension=2, tiled=True)
        .astype(jnp.float32)
        .astype(jnp.bfloat16)
    )
    back = lax.all_to_all(shared_rows, "sp", split_axis=1, concat_axis=0, tiled=True)
    back_flat = back.reshape(experts * capacity, feature_share)
    per_token = back_flat[target].astype(jnp.float32).reshape(tok_rows, top_k, feature_share)
    own_cot = lax.dynamic_slice_in_dim(cotangent, share_offset, feature_share, 1).astype(
        jnp.float32
    )
    residual_grad = (own_cot + jnp.sum(per_token, axis=1)).astype(jnp.bfloat16)
    full_grad = lax.all_gather(residual_grad, "tp", axis=1, tiled=True)
    taps_f = taps.astype(jnp.float32)
    gated = c_gate.astype(jnp.float32) * x_in.astype(jnp.float32)
    earlier = from_behind(gated[tok_rows - 2 :], "sp", 1)
    padded = jnp.concatenate([earlier, gated], axis=0)
    conv = (
        taps_f[0] * padded[0:tok_rows]
        + taps_f[1] * padded[1 : tok_rows + 1]
        + taps_f[2] * padded[2 : tok_rows + 2]
    )
    b_f = b_gate.astype(jnp.float32)
    y_short = (b_f * conv).astype(jnp.bfloat16)
    d_y = jnp.dot(full_grad, w_out, preferred_element_type=jnp.float32)
    grad_b = (d_y * conv).astype(jnp.bfloat16)
    d_conv = b_f * d_y
    following = from_behind(d_conv[0:2], "sp", -1)
    later = jnp.concatenate([d_conv, following], axis=0)
    d_v = (
        taps_f[2] * later[0:tok_rows]
        + taps_f[1] * later[1 : tok_rows + 1]
        + taps_f[0] * later[2 : tok_rows + 2]
    )
    grad_c = (d_v * x_in.astype(jnp.float32)).astype(jnp.bfloat16)
    grad_x = (d_v * c_gate.astype(jnp.float32)).astype(jnp.bfloat16)
    out_proj_grad = lax.psum_scatter(
        jnp.einsum("td,tc->dc", full_grad, y_short, preferred_element_type=jnp.float32),
        "sp",
        scatter_dimension=0,
        tiled=True,
    )
    return (grad_gate, grad_up, grad_down, out_proj_grad, residual_grad, grad_b, grad_c, grad_x)


def solution(mesh):
    return jax.shard_map(
        per_device,
        mesh=mesh,
        in_specs=(
            P("sp", None),
            P("sp", None),
            P("sp", None),
            P("sp", None),
            P("sp", None, "tp"),
            P("sp", None, "tp"),
            P("sp", "tp", None),
            P("sp", "tp"),
            P("sp", "tp"),
            P("sp", "tp"),
            P(None, "tp"),
            P(None, "tp"),
        ),
        out_specs=(
            P("sp", None, "tp"),
            P("sp", None, "tp"),
            P("sp", "tp", None),
            P("sp", "tp"),
            P("sp", "tp"),
            P("sp", "tp"),
            P("sp", "tp"),
            P("sp", "tp"),
        ),
        check_vma=False,
    )
```

profile of v0, /device:TPU:0, one launch (start us, length us, event | category | flops | bytes accessed | tf_op | source)
XLA Modules:
  0.0 290.6 jit_solution(8759638803570472328)
XLA Ops:
  7.2 0.0 all-gather.4.cloned.1.call-start
  7.2 0.8 broadcast_multiply_fusion
  8.0 0.8 copy.30
  8.8 0.1 eq.29
  9.0 0.1 eq.25
  9.1 0.1 copy.29
  9.2 0.1 mul.129
  9.4 1.1 reduce-window.6
  10.6 0.2 slice_reduce_fusion
  10.8 0.1 fusion.56
  10.9 2.4 scatter_custom_fusion
  13.4 0.8 copy.32
  14.2 0.1 reshape.162
  14.4 5.0 %gather_fusion.1 = f32[768]{0:T(1024)S(1)} fusion(f32[512]{0:T(512)S(1)} %reshape.162, s32[1024]{0:T(1024)S(1)} %get-tuple-element.22), kind=kCustom, calls=%fused_computation.1 | custom fusion | bytes 9216 | tf_op jit(solution)/shard_map/gather | solution.py:50
  19.4 0.1 broadcast_in_dim.30
  19.5 1.0 constant_dynamic-slice_fusion.1
  20.5 2.7 gather_fusion
  23.2 0.2 broadcast_select_fusion
  23.3 27.3 %all_to_all.33 = bf16[8,96,512]{2,1,0:T(8,128)(2,1)} all-to-all(bf16[8,96,512]{2,1,0:T(8,128)(2,1)S(1)} %broadcast_select_fusion), channel_id=1, replica_groups=mesh['sp'=8,'tp'=4] {'sp'}, dimensions={0} | all-to-all | bytes 1572864 | tf_op jit(solution)/shard_map/all_to_all | solution.py:58
  50.7 0.0 all-gather.4.cloned.1.call-update
  50.7 0.0 all-gather.6.cloned.1.call-start
  50.7 1.0 constant_dynamic-slice_fusion
  51.7 2.7 gather_fusion.2
  54.4 0.1 mul.132
  54.5 0.2 fusion.31
  54.7 23.3 %all_to_all.34 = bf16[8,96,512]{2,1,0:T(8,128)(2,1)} all-to-all(bf16[8,96,512]{2,1,0:T(8,128)(2,1)S(1)} %fusion.31), channel_id=1, replica_groups=mesh['sp'=8,'tp'=4] {'sp'}, dimensions={0} | all-to-all | bytes 1572864 | tf_op jit(solution)/shard_map/all_to_all | solution.py:59
  78.0 0.0 all-gather.6.cloned.1.call-update
  78.0 0.2 reduce-scatter.3.cloned.1.call-start
  78.3 0.1 all-gather.4.cloned.1.call-done
  78.4 3.9 %fusion.8 = f32[768,256]{1,0:T(8,128)} fusion(bf16[1,768,2048]{2,1,0:T(8,128)(2,1)} %all-gather.4.cloned.1.call-done, bf16[1,2048,256]{2,1,0:T(8,128)(2,1)S(1)} %copy-done), kind=kOutput, calls=%fused_computation.14 | convolution fusion | flops 805306368 | bytes 4980736 | tf_op jit(solution)/shard_map/erd,edf->erf/dot_general | solution.py:65
  82.3 1.9 fusion.10
  84.2 24.3 %all-gather.6.cloned.1.call-done = bf16[1,768,2048]{2,1,0:T(8,128)(2,1)} async-done(((bf16[1,768,512]{2,1,0:T(8,128)(2,1)}), bf16[1,768,2048]{2,1,0:T(8,128)(2,1)}) %all-gather.6.cloned.1.call-update) | async-done | bytes 3145744 | tf_op jit(solution)/shard_map/all_gather | solution.py:63
  108.5 3.5 %multiply_convert_fusion.1 = (bf16[768,256]{1,0:T(8,128)(2,1)S(1)}, bf16[768,256]{1,0:T(8,128)(2,1)S(1)}) fusion(f32[768,256]{1,0:T(8,128)} %fusion.8, f32[768,256]{1,0:T(8,128)} %fusion.10, bf16[1,256,2048]{2,1,0:T(8,128)(2,1)S(1)} %copy-done.14, bf16[1,768,2048]{2,1,0:T(8,128)(2,1)} %all-gather.6.cloned.1.call-done), kind=kOutput, calls=%fused_computation.35 | convolution fusion | flops 807862272 | bytes 6553600 | tf_op jit(solution)/shard_map/erd,efd->erf/dot_general | solution.py:70
  112.0 1.0 fusion.32
  113.0 2.7 fusion.12
  115.8 0.0 reduce-scatter.3.cloned.1.call-update
  115.8 37.9 %reduce-scatter.3.cloned.1.call-done = bf16[1,768,512]{2,1,0:T(8,128)(2,1)} async-done(((bf16[1,768,2048]{2,1,0:T(8,128)(2,1)}), bf16[1,768,512]{2,1,0:T(8,128)(2,1)}) %reduce-scatter.3.cloned.1.call-update) | async-done | bytes 786448 | tf_op jit(solution)/shard_map/reduce_scatter | solution.py:88
  153.7 2.3 copy.38
  156.0 0.5 broadcast.111
  156.5 5.6 %reduce.2 = bf16[768,512]{1,0:T(8,128)(2,1)S(1)} reduce(bf16[768,1,512]{2,1,0:T(2,128)(2,1)S(1)} %bitcast.84, bf16[]{:T(256)} %broadcast.111), dimensions={1}, to_apply=%bitcast.82.reduce_sub_computation | reduce | bytes 1572866
  162.2 1.5 reshape.216
  163.6 5.5 %all-to-all-start.2 = ((bf16[8,2,24576]{2,1,0:T(2,128)(2,1)}), bf16[8,2,24576]{2,1,0:T(2,128)(2,1)S(1)}, u32[]{:S(2)}, u32[]{:S(2)}) async-start(bf16[8,2,24576]{2,1,0:T(2,128)(2,1)} %reshape.216), calls=%async_computation.3 | async-start | bytes 1572864 | tf_op jit(solution)/shard_map/all_to_all | solution.py:92
  169.1 0.3 all-gather.8.cloned.1.call-start
  169.4 19.8 %all-to-all-done.2 = bf16[8,2,24576]{2,1,0:T(2,128)(2,1)S(1)} async-done(((bf16[8,2,24576]{2,1,0:T(2,128)(2,1)}), bf16[8,2,24576]{2,1,0:T(2,128)(2,1)S(1)}, u32[]{:S(2)}, u32[]{:S(2)}) %all-to-all-start.2) | async-done | bytes 786464 | tf_op jit(solution)/shard_map/all_to_all | solution.py:92
  189.2 0.8 reshape.217
  190.0 0.2 copy.37
  190.2 2.0 gather_fusion.3
  192.3 0.7 reshape.169
  192.9 1.2 reduce_sum.22
  194.2 1.7 add_convert_fusion.1
  195.9 0.0 reduce-scatter.5.cloned.1.call-start
  196.0 3.2 %collective-permute-start = (f32[2,256]{1,0:T(2,128)S(1)}, f32[2,256]{1,0:T(2,128)S(1)}, u32[]{:S(2)}, u32[]{:S(2)}) collective-permute-start(f32[2,256]{1,0:T(2,128)S(1)} %slice.57), channel_id=1, source_target_pairs={{0,4},{4,8},{8,12},{12,16},{16,20},{20,24},{24,28},{1,5},{5,9},{9,... | collective-permute-start | bytes 6152 | tf_op jit(solution)/shard_map/ppermute | solution.py:10
  199.3 1.3 collective-permute-done
  200.6 10.2 %all-gather.8.cloned.1.call-done = bf16[256,2048]{1,0:T(8,128)(2,1)} async-done(((bf16[256,512]{1,0:T(8,128)(2,1)}), bf16[256,2048]{1,0:T(8,128)(2,1)}) %all-gather.8.cloned.1.call-update) | async-done | bytes 1048592 | tf_op jit(solution)/shard_map/all_gather | solution.py:99
  210.8 2.7 multiply_convert_fusion.4
  213.5 1.8 fusion.53
  215.4 4.1 %fusion.28 = bf16[1,2048,256]{2,1,0:T(8,128)(2,1)} fusion(bf16[768,256]{1,0:T(8,128)(2,1)S(1)} %copy-done.2, bf16[1,768,2048]{2,1,0:T(8,128)(2,1)} %all-gather.4.cloned.1.call-done), kind=kOutput, calls=%fused_computation.24 | convolution fusion | flops 805830656 | bytes 4587520 | tf_op jit(solution)/shard_map/erd,erf->edf/dot_general | solution.py:76
  219.5 2.0 fusion.22
  221.5 1.3 collective-permute-start.1
  222.9 2.0 fusion.25
  224.9 2.3 collective-permute-done.1
  227.2 0.8 fusion.48
  227.9 0.7 fusion.49
  228.6 55.5 %reduce-scatter.5.cloned.1.call-done = f32[256,256]{1,0:T(8,128)} async-done(((f32[2048,256]{1,0:T(8,128)}), f32[256,256]{1,0:T(8,128)}) %reduce-scatter.5.cloned.1.call-update) | async-done | bytes 262160 | tf_op jit(solution)/shard_map/reduce_scatter | solution.py:123
  (49 shorter events, 0.2 us)
Async XLA Ops:
  7.2 71.2 %copy-start = (bf16[1,2048,256]{2,1,0:T(8,128)(2,1)S(1)}, bf16[1,2048,256]{2,1,0:T(8,128)(2,1)}, u32[]{:S(2)}) copy-start(bf16[1,2048,256]{2,1,0:T(8,128)(2,1)} %param.16) | copy-start | bytes 3145732
  7.2 71.2 %all-gather.4.cloned.1.call-start = ((), (), s32[]{:S(2)}) async-start(), calls=%async_computation.5 | async-start | bytes 3932160 | tf_op jit(solution)/shard_map/all_gather | solution.py:62
  50.7 57.8 %all-gather.6.cloned.1.call-start = ((), (), s32[]{:S(2)}) async-start(), calls=%async_computation.6 | async-start | bytes 3932160 | tf_op jit(solution)/shard_map/all_gather | solution.py:63
  78.0 4.3 %copy-start.4 = (bf16[1,2048,256]{2,1,0:T(8,128)(2,1)S(1)}, bf16[1,2048,256]{2,1,0:T(8,128)(2,1)}, u32[]{:S(2)}) copy-start(bf16[1,2048,256]{2,1,0:T(8,128)(2,1)} %param.17) | copy-start | bytes 3145732
  78.0 75.6 %reduce-scatter.3.cloned.1.call-start = ((), (), s32[]{:S(2)}) async-start(), calls=%async_computation.7 | async-start | bytes 3932160 | tf_op jit(solution)/shard_map/reduce_scatter | solution.py:88
  78.4 3.9 %copy-start.11 = (bf16[1,768,2048]{2,1,0:T(8,128)(2,1)S(1)}, bf16[1,768,2048]{2,1,0:T(8,128)(2,1)}, u32[]{:S(2)}) copy-start(bf16[1,768,2048]{2,1,0:T(8,128)(2,1)} %all-gather.4.cloned.1.call-done) | copy-start | bytes 9437188
  82.3 26.2 %copy-start.14 = (bf16[1,256,2048]{2,1,0:T(8,128)(2,1)S(1)}, bf16[1,256,2048]{2,1,0:T(8,128)(2,1)}, u32[]{:S(2)}) copy-start(bf16[1,256,2048]{2,1,0:T(8,128)(2,1)} %param.18) | copy-start | bytes 3145732
  112.0 1.0 copy-start.1
  112.0 1.0 copy-start.7
  163.6 25.6 %all-to-all-start.2 = ((bf16[8,2,24576]{2,1,0:T(2,128)(2,1)}), bf16[8,2,24576]{2,1,0:T(2,128)(2,1)S(1)}, u32[]{:S(2)}, u32[]{:S(2)}) async-start(bf16[8,2,24576]{2,1,0:T(2,128)(2,1)} %reshape.216), calls=%async_computation.3 | async-start | bytes 1572864 | tf_op jit(solution)/shard_map/all_to_all | solution.py:92
  169.1 41.6 %all-gather.8.cloned.1.call-start = ((), (), s32[]{:S(2)}) async-start(), calls=%async_computation.8 | async-start | bytes 1310720 | tf_op jit(solution)/shard_map/all_gather | solution.py:99
  192.2 3.8 %copy-start.5 = (bf16[256,256]{1,0:T(8,128)(2,1)S(1)}, bf16[256,256]{1,0:T(8,128)(2,1)}, u32[]{:S(2)}) copy-start(bf16[256,256]{1,0:T(8,128)(2,1)} %param.20) | copy-start | bytes 393220
  192.2 3.8 %copy-start.6 = (bf16[256,256]{1,0:T(8,128)(2,1)S(1)}, bf16[256,256]{1,0:T(8,128)(2,1)}, u32[]{:S(2)}) copy-start(bf16[256,256]{1,0:T(8,128)(2,1)} %param.21) | copy-start | bytes 393220
  192.2 7.0 %copy-start.10 = (bf16[3,256]{1,0:T(4,128)(2,1)S(1)}, bf16[3,256]{1,0:T(4,128)(2,1)}, u32[]{:S(2)}) copy-start(bf16[3,256]{1,0:T(4,128)(2,1)} %param.22) | copy-start | bytes 4612
  192.3 18.5 %copy-start.9 = (bf16[256,256]{1,0:T(8,128)(2,1)S(1)}, bf16[256,256]{1,0:T(8,128)(2,1)}, u32[]{:S(2)}) copy-start(bf16[256,256]{1,0:T(8,128)(2,1)} %param.19) | copy-start | bytes 393220
  195.9 88.1 %reduce-scatter.5.cloned.1.call-start = ((), (), s32[]{:S(2)}) async-start(), calls=%async_computation.9 | async-start | bytes 2359296 | tf_op jit(solution)/shard_map/reduce_scatter | solution.py:123
  196.0 4.5 %collective-permute-start = (f32[2,256]{1,0:T(2,128)S(1)}, f32[2,256]{1,0:T(2,128)S(1)}, u32[]{:S(2)}, u32[]{:S(2)}) collective-permute-start(f32[2,256]{1,0:T(2,128)S(1)} %slice.57), channel_id=1, source_target_pairs={{0,4},{4,8},{8,12},{12,16},{16,20},{20,24},{24,28},{1,5},{5,9},{9,... | collective-permute-start | bytes 6152 | tf_op jit(solution)/shard_map/ppermute | solution.py:10
  210.8 2.7 copy-start.3
  213.5 1.9 copy-start.2
  215.4 4.1 %copy-start.13 = (bf16[1,768,2048]{2,1,0:T(8,128)(2,1)S(1)}, bf16[1,768,2048]{2,1,0:T(8,128)(2,1)}, u32[]{:S(2)}) copy-start(bf16[1,768,2048]{2,1,0:T(8,128)(2,1)} %all-gather.6.cloned.1.call-done) | copy-start | bytes 9437188
  215.4 4.1 %copy-start.15 = (f32[768,256]{1,0:T(8,128)S(1)}, f32[768,256]{1,0:T(8,128)}, u32[]{:S(2)}) copy-start(f32[768,256]{1,0:T(8,128)} %fusion.8) | copy-start | bytes 2359300
  215.4 4.1 %copy-start.16 = (f32[768,256]{1,0:T(8,128)S(1)}, f32[768,256]{1,0:T(8,128)}, u32[]{:S(2)}) copy-start(f32[768,256]{1,0:T(8,128)} %fusion.10) | copy-start | bytes 2359300
  219.5 3.3 %copy-start.8 = (bf16[768,256]{1,0:T(8,128)(2,1)S(1)}, bf16[768,256]{1,0:T(8,128)(2,1)}, u32[]{:S(2)}) copy-start(bf16[768,256]{1,0:T(8,128)(2,1)} %copy-done.7) | copy-start | bytes 1179652
  219.5 3.3 %copy-start.12 = (bf16[1,768,2048]{2,1,0:T(8,128)(2,1)S(1)}, bf16[1,768,2048]{2,1,0:T(8,128)(2,1)}, u32[]{:S(2)}) copy-start(bf16[1,768,2048]{2,1,0:T(8,128)(2,1)} %all-gather.4.cloned.1.call-done) | copy-start | bytes 9437188
  221.5 5.6 %collective-permute-start.1 = (f32[2,256]{1,0:T(2,128)S(1)}, f32[2,256]{1,0:T(2,128)S(1)}, u32[]{:S(2)}, u32[]{:S(2)}) collective-permute-start(f32[2,256]{1,0:T(2,128)S(1)} %slice.62), channel_id=1, source_target_pairs={{4,0},{8,4},{12,8},{16,12},{20,16},{24,20},{28,24},{5,1},{9,5},{13... | collective-permute-start | bytes 6152 | tf_op jit(solution)/shard_map/ppermute | solution.py:10
Sparse Core Ops, SparseCore 0:
  50.8 27.5 all-gather.3
  80.0 28.4 all-gather.5
  115.9 37.7 reduce-scatter.2
  196.1 14.6 all-gather.7
  215.5 68.5 reduce-scatter.4
where the time goes:
time: 291 us
  waiting for transfers between devices  151 us (52%)
  blocking collectives  50.6 us (17%)
  matrix products  25.7 us (9%)
  local copies, waits for them, and re-layouts  25.5 us (9%)
  between operations  14.2 us (5%)
  other arithmetic  12.6 us (4%)
  starting transfers between devices  10.6 us (4%)
    reduce_scatter x1, waiting for transfers between devices, per_device(): lax.psum_scatter(jnp.einsum('td,tc->dc', full_grad, y_short, preferred_el...  55.5 us
    reduce_scatter x1, waiting for transfers between devices, per_device(): lax.psum_scatter(partial_low, 'tp', scatter_dimension=2, tiled=True)  37.9 us
    all_to_all x1, blocking collectives, per_device(): lax.all_to_all(send_rows, 'sp', split_axis=0, concat_axis=1, tiled=True)  27.3 us
    all_gather x1, waiting for transfers between devices, per_device(): lax.all_gather(part_cot, 'tp', axis=2, tiled=True)  24.3 us
    all_to_all x1, blocking collectives, per_device(): lax.all_to_all(send_cot, 'sp', split_axis=0, concat_axis=1, tiled=True)  23.3 us
    all_to_all x1, waiting for transfers between devices, per_device(): lax.all_to_all(shared_rows, 'sp', split_axis=1, concat_axis=0, tiled=True)  19.8 us
    all_gather x1, waiting for transfers between devices, per_device(): full_grad = lax.all_gather(residual_grad, 'tp', axis=1, tiled=True)  10.2 us
  transfers between devices with their start and end apart: 8, of which 8 were waited for; matrix products, arithmetic and copies ran while one was open for 7% of the time, Pallas kernels for 0%

commit v1 on v0

--- a/solution.py
+++ b/solution.py
@@ -60,7 +60,9 @@
     )
     rows_h, rows_s = (
         lax.all_gather(part_rows, "tp", axis=2, tiled=True),
-        lax.all_gather(part_cot, "tp", axis=2, tiled=True),
+        jnp.concatenate(
+            lax.all_to_all(jnp.stack([part_cot] * lax.axis_size("tp")), "tp", 0, 0), axis=2
+        ),
     )
     pre_gate = jnp.einsum("erd,edf->erf", rows_h, w_gate, preferred_element_type=jnp.float32)
     pre_up = jnp.einsum("erd,edf->erf", rows_h, w_up, preferred_element_type=jnp.float32)

time: 291 us -> 302 us (1.038)
  starting transfers between devices: 10.6 us -> 15.2 us
    all_to_all x0 -> x1, waiting for transfers between devices: none -> 30.9 us  [per_device(): lax.all_to_all(jnp.stack([part_cot] * lax.axis_size('tp')), 'tp', 0, 0)]
    all_gather x1 -> x0, waiting for transfers between devices: 24.3 us -> none  [per_device(): lax.all_gather(part_cot, 'tp', axis=2, tiled=True)]
    all_to_all x0 -> x1, starting transfers between devices: none -> 4.66 us  [per_device(): lax.all_to_all(jnp.stack([part_cot] * lax.axis_size('tp')), 'tp', 0, 0)]
  transfers between devices with their start and end apart: 8 -> 8, of which waited for: 8 -> 7; matrix products, arithmetic and copies ran while one was open for 7% -> 8% of each run, Pallas kernels for 0% -> 0%
where the time goes in v1:
time: 302 us
  waiting for transfers between devices  154 us (51%)
  blocking collectives  50.5 us (17%)
  local copies, waits for them, and re-layouts  27.7 us (9%)
  matrix products  27.7 us (9%)
  starting transfers between devices  15.2 us (5%)
  between operations  14.2 us (5%)
  other arithmetic  12.6 us (4%)
    reduce_scatter x1, waiting for transfers between devices, per_device(): lax.psum_scatter(jnp.einsum('td,tc->dc', full_grad, y_short, preferred_el...  53.4 us
    reduce_scatter x1, waiting for transfers between devices, per_device(): lax.psum_scatter(partial_low, 'tp', scatter_dimension=2, tiled=True)  35.9 us
    all_to_all x1, waiting for transfers between devices, per_device(): lax.all_to_all(jnp.stack([part_cot] * lax.axis_size('tp')), 'tp', 0, 0)  30.9 us
    all_to_all x1, blocking collectives, per_device(): lax.all_to_all(send_rows, 'sp', split_axis=0, concat_axis=1, tiled=True)  27.3 us
    all_to_all x1, blocking collectives, per_device(): lax.all_to_all(send_cot, 'sp', split_axis=0, concat_axis=1, tiled=True)  23.2 us
    all_to_all x1, waiting for transfers between devices, per_device(): lax.all_to_all(shared_rows, 'sp', split_axis=1, concat_axis=0, tiled=True)  19.8 us
    all_gather x1, waiting for transfers between devices, per_device(): full_grad = lax.all_gather(residual_grad, 'tp', axis=1, tiled=True)  10.2 us
  transfers between devices with their start and end apart: 8, of which 7 were waited for; matrix products, arithmetic and copies ran while one was open for 8% of the time, Pallas kernels for 0%

profile of v1, /device:TPU:0, one launch (start us, length us, event | category | flops | bytes accessed | tf_op | source)
XLA Modules:
  0.0 301.7 jit_solution(3290082321231452155)
XLA Ops:
  7.2 0.0 all-gather.3.cloned.1.call-start
  7.2 0.8 broadcast_multiply_fusion
  8.0 0.8 copy.33
  8.8 0.1 eq.29
  9.0 0.1 eq.25
  9.1 0.1 copy.32
  9.2 0.1 mul.129
  9.4 1.1 reduce-window.6
  10.6 0.2 slice_reduce_fusion
  10.8 0.1 fusion.48
  10.9 2.4 scatter_custom_fusion
  13.4 0.8 copy.35
  14.2 0.1 reshape.173
  14.4 5.0 %gather_fusion.1 = f32[768]{0:T(1024)S(1)} fusion(f32[512]{0:T(512)S(1)} %reshape.173, s32[1024]{0:T(1024)S(1)} %get-tuple-element.22), kind=kCustom, calls=%fused_computation.1 | custom fusion | bytes 9216 | tf_op jit(solution)/shard_map/gather | solution.py:50
  19.4 0.1 broadcast_in_dim.30
  19.5 1.0 constant_dynamic-slice_fusion.1
  20.5 2.7 gather_fusion
  23.2 0.2 broadcast_select_fusion
  23.3 27.3 %all_to_all.35 = bf16[8,96,512]{2,1,0:T(8,128)(2,1)} all-to-all(bf16[8,96,512]{2,1,0:T(8,128)(2,1)S(1)} %broadcast_select_fusion), channel_id=1, replica_groups=mesh['sp'=8,'tp'=4] {'sp'}, dimensions={0} | all-to-all | bytes 1572864 | tf_op jit(solution)/shard_map/all_to_all | solution.py:58
  50.7 0.0 all-gather.3.cloned.1.call-update
  50.7 1.0 constant_dynamic-slice_fusion
  51.7 2.7 gather_fusion.2
  54.4 0.1 mul.132
  54.4 0.2 fusion.22
  54.7 23.2 %all_to_all.36 = bf16[8,96,512]{2,1,0:T(8,128)(2,1)S(1)} all-to-all(bf16[8,96,512]{2,1,0:T(8,128)(2,1)S(1)} %fusion.22), channel_id=1, replica_groups=mesh['sp'=8,'tp'=4] {'sp'}, dimensions={0} | all-to-all | bytes 1572864 | tf_op jit(solution)/shard_map/all_to_all | solution.py:59
  77.9 0.3 copy.36
  78.1 1.9 stack.10
  80.1 4.7 %all-to-all-start.2 = ((bf16[4,1,768,512]{2,3,1,0:T(8,128)(2,1)}), bf16[4,1,768,512]{2,3,1,0:T(8,128)(2,1)}, u32[]{:S(2)}, u32[]{:S(2)}) async-start(bf16[4,1,768,512]{2,3,1,0:T(8,128)(2,1)} %stack.10), calls=%async_computation.2 | async-start | bytes 6291456 | tf_op jit(solution)/shard_map/all_to_all | solution.py:64
  84.7 0.2 reduce-scatter.3.cloned.1.call-start
  85.0 0.0 all-gather.3.cloned.1.call-done
  85.0 3.9 %fusion.4 = f32[768,256]{1,0:T(8,128)} fusion(bf16[1,768,2048]{2,1,0:T(8,128)(2,1)} %all-gather.3.cloned.1.call-done, bf16[1,2048,256]{2,1,0:T(8,128)(2,1)S(1)} %copy-done), kind=kOutput, calls=%fused_computation.10 | convolution fusion | flops 805306368 | bytes 4980736 | tf_op jit(solution)/shard_map/erd,edf->erf/dot_general | solution.py:67
  88.9 1.9 fusion.6
  90.8 30.9 %all-to-all-done.2 = bf16[4,1,768,512]{2,3,1,0:T(8,128)(2,1)} async-done(((bf16[4,1,768,512]{2,3,1,0:T(8,128)(2,1)}), bf16[4,1,768,512]{2,3,1,0:T(8,128)(2,1)}, u32[]{:S(2)}, u32[]{:S(2)}) %all-to-all-start.2) | async-done | bytes 3145760 | tf_op jit(solution)/shard_map/all_to_all | solution.py:64
  121.7 3.5 %multiply_convert_fusion.1 = (bf16[768,256]{1,0:T(8,128)(2,1)S(1)}, bf16[768,256]{1,0:T(8,128)(2,1)S(1)}) fusion(f32[768,256]{1,0:T(8,128)} %fusion.4, f32[768,256]{1,0:T(8,128)} %fusion.6, bf16[768,2048]{0,1:T(8,128)(2,1)} %bitcast.11, bf16[1,256,2048]{2,1,0:T(8,128)(2,1)S(1)} %copy-done.13), kind=kOutput, calls=%fused_computation.32 | convolution fusion | flops 807862272 | bytes 6553600 | tf_op jit(solution)/shard_map/erd,efd->erf/dot_general | solution.py:72
  125.2 1.0 fusion.23
  126.2 2.7 fusion.8
  129.0 35.9 %reduce-scatter.3.cloned.1.call-done = bf16[1,768,512]{2,1,0:T(8,128)(2,1)} async-done(((bf16[1,768,2048]{2,1,0:T(8,128)(2,1)}), bf16[1,768,512]{2,1,0:T(8,128)(2,1)}) %reduce-scatter.3.cloned.1.call-update) | async-done | bytes 786448 | tf_op jit(solution)/shard_map/reduce_scatter | solution.py:90
  165.0 2.3 copy.43
  167.3 0.5 broadcast.113
  167.8 5.6 %reduce.2 = bf16[768,512]{1,0:T(8,128)(2,1)S(1)} reduce(bf16[768,1,512]{2,1,0:T(2,128)(2,1)S(1)} %bitcast.80, bf16[]{:T(256)} %broadcast.113), dimensions={1}, to_apply=%bitcast.78.reduce_sub_computation | reduce | bytes 1572866
  173.5 1.5 reshape.228
  174.9 5.5 %all-to-all-start.3 = ((bf16[8,2,24576]{2,1,0:T(2,128)(2,1)}), bf16[8,2,24576]{2,1,0:T(2,128)(2,1)S(1)}, u32[]{:S(2)}, u32[]{:S(2)}) async-start(bf16[8,2,24576]{2,1,0:T(2,128)(2,1)} %reshape.228), calls=%async_computation.4 | async-start | bytes 1572864 | tf_op jit(solution)/shard_map/all_to_all | solution.py:94
  180.4 0.3 all-gather.5.cloned.1.call-start
  180.7 19.8 %all-to-all-done.3 = bf16[8,2,24576]{2,1,0:T(2,128)(2,1)S(1)} async-done(((bf16[8,2,24576]{2,1,0:T(2,128)(2,1)}), bf16[8,2,24576]{2,1,0:T(2,128)(2,1)S(1)}, u32[]{:S(2)}, u32[]{:S(2)}) %all-to-all-start.3) | async-done | bytes 786464 | tf_op jit(solution)/shard_map/all_to_all | solution.py:94
  200.5 0.8 reshape.229
  201.3 0.2 copy.42
  201.5 2.0 gather_fusion.3
  203.6 0.7 reshape.181
  204.2 1.2 reduce_sum.22
  205.5 1.7 add_convert_fusion.1
  207.2 0.0 reduce-scatter.5.cloned.1.call-start
  207.3 3.2 %collective-permute-start = (f32[2,256]{1,0:T(2,128)S(1)}, f32[2,256]{1,0:T(2,128)S(1)}, u32[]{:S(2)}, u32[]{:S(2)}) collective-permute-start(f32[2,256]{1,0:T(2,128)S(1)} %slice.57), channel_id=1, source_target_pairs={{0,4},{4,8},{8,12},{12,16},{16,20},{20,24},{24,28},{1,5},{5,9},{9,... | collective-permute-start | bytes 6152 | tf_op jit(solution)/shard_map/ppermute | solution.py:10
  210.6 1.3 collective-permute-done
  211.9 10.2 %all-gather.5.cloned.1.call-done = bf16[256,2048]{1,0:T(8,128)(2,1)} async-done(((bf16[256,512]{1,0:T(8,128)(2,1)}), bf16[256,2048]{1,0:T(8,128)(2,1)}) %all-gather.5.cloned.1.call-update) | async-done | bytes 1048592 | tf_op jit(solution)/shard_map/all_gather | solution.py:101
  222.1 2.7 multiply_convert_fusion.4
  224.8 1.8 fusion.45
  226.7 4.0 %fusion.19 = bf16[1,2048,256]{2,1,0:T(8,128)(2,1)} fusion(bf16[768,256]{1,0:T(8,128)(2,1)S(1)} %copy-done.2, bf16[1,768,2048]{2,1,0:T(8,128)(2,1)} %all-gather.3.cloned.1.call-done), kind=kOutput, calls=%fused_computation.20 | convolution fusion | flops 805830656 | bytes 4587520 | tf_op jit(solution)/shard_map/erd,erf->edf/dot_general | solution.py:78
  230.7 4.1 %fusion.15 = bf16[1,256,2048]{2,1,0:T(8,128)(2,1)} fusion(bf16[768,2048]{0,1:T(8,128)(2,1)} %bitcast.11, f32[768,256]{1,0:T(8,128)S(1)} %copy-done.15, f32[768,256]{1,0:T(8,128)S(1)} %copy-done.14), kind=kOutput, calls=%fused_computation.18 | convolution fusion | flops 807010304 | bytes 5767168 | tf_op jit(solution)/shard_map/erf,erd->efd/dot_general | solution.py:75
  234.8 1.3 collective-permute-start.1
  236.1 2.0 fusion.16
  238.2 2.1 collective-permute-done.1
  240.3 0.8 fusion.40
  241.0 0.7 fusion.41
  241.7 53.4 %reduce-scatter.5.cloned.1.call-done = f32[256,256]{1,0:T(8,128)} async-done(((f32[2048,256]{1,0:T(8,128)}), f32[256,256]{1,0:T(8,128)}) %reduce-scatter.5.cloned.1.call-update) | async-done | bytes 262160 | tf_op jit(solution)/shard_map/reduce_scatter | solution.py:125
  (48 shorter events, 0.3 us)
Async XLA Ops:
  7.2 77.8 %copy-start = (bf16[1,2048,256]{2,1,0:T(8,128)(2,1)S(1)}, bf16[1,2048,256]{2,1,0:T(8,128)(2,1)}, u32[]{:S(2)}) copy-start(bf16[1,2048,256]{2,1,0:T(8,128)(2,1)} %param.16) | copy-start | bytes 3145732
  7.2 77.8 %all-gather.3.cloned.1.call-start = ((), (), s32[]{:S(2)}) async-start(), calls=%async_computation.6 | async-start | bytes 3932160 | tf_op jit(solution)/shard_map/all_gather | solution.py:62
  80.1 41.6 %all-to-all-start.2 = ((bf16[4,1,768,512]{2,3,1,0:T(8,128)(2,1)}), bf16[4,1,768,512]{2,3,1,0:T(8,128)(2,1)}, u32[]{:S(2)}, u32[]{:S(2)}) async-start(bf16[4,1,768,512]{2,3,1,0:T(8,128)(2,1)} %stack.10), calls=%async_computation.2 | async-start | bytes 6291456 | tf_op jit(solution)/shard_map/all_to_all | solution.py:64
  84.7 4.2 %copy-start.4 = (bf16[1,2048,256]{2,1,0:T(8,128)(2,1)S(1)}, bf16[1,2048,256]{2,1,0:T(8,128)(2,1)}, u32[]{:S(2)}) copy-start(bf16[1,2048,256]{2,1,0:T(8,128)(2,1)} %param.17) | copy-start | bytes 3145732
  84.7 80.2 %reduce-scatter.3.cloned.1.call-start = ((), (), s32[]{:S(2)}) async-start(), calls=%async_computation.7 | async-start | bytes 3932160 | tf_op jit(solution)/shard_map/reduce_scatter | solution.py:90
  85.0 3.9 %copy-start.11 = (bf16[1,768,2048]{2,1,0:T(8,128)(2,1)S(1)}, bf16[1,768,2048]{2,1,0:T(8,128)(2,1)}, u32[]{:S(2)}) copy-start(bf16[1,768,2048]{2,1,0:T(8,128)(2,1)} %all-gather.3.cloned.1.call-done) | copy-start | bytes 9437188
  88.9 32.8 %copy-start.13 = (bf16[1,256,2048]{2,1,0:T(8,128)(2,1)S(1)}, bf16[1,256,2048]{2,1,0:T(8,128)(2,1)}, u32[]{:S(2)}) copy-start(bf16[1,256,2048]{2,1,0:T(8,128)(2,1)} %param.18) | copy-start | bytes 3145732
  125.2 1.0 copy-start.1
  125.2 1.0 copy-start.7
  174.9 25.6 %all-to-all-start.3 = ((bf16[8,2,24576]{2,1,0:T(2,128)(2,1)}), bf16[8,2,24576]{2,1,0:T(2,128)(2,1)S(1)}, u32[]{:S(2)}, u32[]{:S(2)}) async-start(bf16[8,2,24576]{2,1,0:T(2,128)(2,1)} %reshape.228), calls=%async_computation.4 | async-start | bytes 1572864 | tf_op jit(solution)/shard_map/all_to_all | solution.py:94
  180.4 41.6 %all-gather.5.cloned.1.call-start = ((), (), s32[]{:S(2)}) async-start(), calls=%async_computation.8 | async-start | bytes 1310720 | tf_op jit(solution)/shard_map/all_gather | solution.py:101
  203.5 3.8 %copy-start.5 = (bf16[256,256]{1,0:T(8,128)(2,1)S(1)}, bf16[256,256]{1,0:T(8,128)(2,1)}, u32[]{:S(2)}) copy-start(bf16[256,256]{1,0:T(8,128)(2,1)} %param.20) | copy-start | bytes 393220
  203.5 3.8 %copy-start.6 = (bf16[256,256]{1,0:T(8,128)(2,1)S(1)}, bf16[256,256]{1,0:T(8,128)(2,1)}, u32[]{:S(2)}) copy-start(bf16[256,256]{1,0:T(8,128)(2,1)} %param.21) | copy-start | bytes 393220
  203.5 7.0 %copy-start.10 = (bf16[3,256]{1,0:T(4,128)(2,1)S(1)}, bf16[3,256]{1,0:T(4,128)(2,1)}, u32[]{:S(2)}) copy-start(bf16[3,256]{1,0:T(4,128)(2,1)} %param.22) | copy-start | bytes 4612
  203.6 18.5 %copy-start.9 = (bf16[256,256]{1,0:T(8,128)(2,1)S(1)}, bf16[256,256]{1,0:T(8,128)(2,1)}, u32[]{:S(2)}) copy-start(bf16[256,256]{1,0:T(8,128)(2,1)} %param.19) | copy-start | bytes 393220
  207.2 87.9 %reduce-scatter.5.cloned.1.call-start = ((), (), s32[]{:S(2)}) async-start(), calls=%async_computation.9 | async-start | bytes 2359296 | tf_op jit(solution)/shard_map/reduce_scatter | solution.py:125
  207.3 4.5 %collective-permute-start = (f32[2,256]{1,0:T(2,128)S(1)}, f32[2,256]{1,0:T(2,128)S(1)}, u32[]{:S(2)}, u32[]{:S(2)}) collective-permute-start(f32[2,256]{1,0:T(2,128)S(1)} %slice.57), channel_id=1, source_target_pairs={{0,4},{4,8},{8,12},{12,16},{16,20},{20,24},{24,28},{1,5},{5,9},{9,... | collective-permute-start | bytes 6152 | tf_op jit(solution)/shard_map/ppermute | solution.py:10
  222.1 2.7 copy-start.3
  224.8 1.9 copy-start.2
  226.7 4.0 %copy-start.14 = (f32[768,256]{1,0:T(8,128)S(1)}, f32[768,256]{1,0:T(8,128)}, u32[]{:S(2)}) copy-start(f32[768,256]{1,0:T(8,128)} %fusion.4) | copy-start | bytes 2359300
  226.7 4.0 %copy-start.15 = (f32[768,256]{1,0:T(8,128)S(1)}, f32[768,256]{1,0:T(8,128)}, u32[]{:S(2)}) copy-start(f32[768,256]{1,0:T(8,128)} %fusion.6) | copy-start | bytes 2359300
  230.7 5.4 %copy-start.8 = (bf16[768,256]{1,0:T(8,128)(2,1)S(1)}, bf16[768,256]{1,0:T(8,128)(2,1)}, u32[]{:S(2)}) copy-start(bf16[768,256]{1,0:T(8,128)(2,1)} %copy-done.7) | copy-start | bytes 1179652
  230.7 5.4 %copy-start.12 = (bf16[1,768,2048]{2,1,0:T(8,128)(2,1)S(1)}, bf16[1,768,2048]{2,1,0:T(8,128)(2,1)}, u32[]{:S(2)}) copy-start(bf16[1,768,2048]{2,1,0:T(8,128)(2,1)} %all-gather.3.cloned.1.call-done) | copy-start | bytes 9437188
  234.8 5.5 %collective-permute-start.1 = (f32[2,256]{1,0:T(2,128)S(1)}, f32[2,256]{1,0:T(2,128)S(1)}, u32[]{:S(2)}, u32[]{:S(2)}) collective-permute-start(f32[2,256]{1,0:T(2,128)S(1)} %slice.62), channel_id=1, source_target_pairs={{4,0},{8,4},{12,8},{16,12},{20,16},{24,20},{28,24},{5,1},{9,5},{13... | collective-permute-start | bytes 6152 | tf_op jit(solution)/shard_map/ppermute | solution.py:10
Sparse Core Ops, SparseCore 0:
  50.8 27.5 all-gather.2
  129.1 35.7 reduce-scatter.2
  207.3 14.6 all-gather.4
  226.8 68.3 reduce-scatter.4
